TPU v7x, 32 devices: a whole 2x2x4 slice. The times are simulated.
32 devices in a mesh: fs: 8 (over z, y), tp: 4 (over x, core).
Axes of the slice: x: 2, y: 2, z: 4, core: 2. Of those that a mesh axis runs over, the one named last changes fastest.
Arguments:
- prompt_tokens: bfloat16 [768, 4096], P('tp'), may hold values from -6 to 6
- norm_gain: float32 [4096], P('fs'), may hold values from 0.1 to 1.9
- gate_trained: float32 [4096, 11264], P('fs', 'tp'), may hold values from -0.09375 to 0.09375
- up_trained: float32 [4096, 11264], P('fs', 'tp'), may hold values from -0.09375 to 0.09375
- down_trained: float32 [11264, 4096], P('fs', 'tp'), may hold values from -0.078125 to 0.078125
Outputs:
- gate_serving: bfloat16 [4096, 11264], P(None, 'fs')
- up_serving: bfloat16 [4096, 11264], P(None, 'fs')
- down_serving: bfloat16 [11264, 4096], P('fs')
- mixed: bfloat16 [768, 4096], P('tp', 'fs')
All inputs are finite; a program needn't handle non-finite values.
Results may differ from a plain program's by a relative error of at most 0.0082.
Values may be sent and summed in bfloat16 or wider, within the bound.
A program may use at most 128 MiB of HBM per device.

v0:
```python
import jax
import jax.numpy as jnp
from jax import lax
from jax.sharding import PartitionSpec as P


def on_device(prompt_tokens, norm_gain, gate_trained, up_trained, down_trained):
    fs_count = lax.axis_size("fs")
    gate_cast = (gate_trained * norm_gain[:, None]).astype(jnp.bfloat16)
    up_cast = (up_trained * norm_gain[:, None]).astype(jnp.bfloat16)
    down_cast = down_trained.astype(jnp.bfloat16)
    down_serving = lax.all_gather(down_cast, "tp", axis=1, tiled=True)
    gate_part, up_part = (
        lax.all_to_all(gate_cast, "tp", split_axis=0, concat_axis=1, tiled=True),
        lax.all_to_all(up_cast, "tp", split_axis=0, concat_axis=1, tiled=True),
    )
    gate_mid, up_mid = (
        lax.all_to_all(gate_part, "fs", split_axis=1, concat_axis=0, tiled=True),
        lax.all_to_all(up_part, "fs", split_axis=1, concat_axis=0, tiled=True),
    )
    share = gate_mid.shape[0] // fs_count
    width = gate_mid.shape[1]
    gate_blocks, up_blocks = (
        lax.all_gather(gate_mid.reshape(fs_count, share, width), "tp", axis=1, tiled=True),
        lax.all_gather(up_mid.reshape(fs_count, share, width), "tp", axis=1, tiled=True),
    )
    gate_serving = gate_blocks.reshape(-1, width)
    up_serving = up_blocks.reshape(-1, width)
    tokens = prompt_tokens.astype(jnp.float32)
    scale = lax.rsqrt(jnp.mean(tokens * tokens, axis=-1, keepdims=True) + 1e-06)
    normed = (tokens * scale).astype(jnp.bfloat16)
    contract = (((0,), (1,)), ((), ()))
    gate_cols = lax.dot_general(gate_serving, normed, contract, preferred_element_type=jnp.float32)
    up_cols = lax.dot_general(up_serving, normed, contract, preferred_element_type=jnp.float32)
    hidden_cols = (jax.nn.silu(gate_cols) * up_cols).astype(jnp.bfloat16)
    summed = lax.psum_scatter(
        lax.dot_general(
            down_serving, hidden_cols, (((0,), (0,)), ((), ())), preferred_element_type=jnp.float32
        ),
        "fs",
        scatter_dimension=0,
        tiled=True,
    )
    mixed = summed.T.astype(jnp.bfloat16)
    return (gate_serving, up_serving, down_serving, mixed)


def solution(mesh):
    return jax.shard_map(
        on_device,
        mesh=mesh,
        in_specs=(P("tp", None), P("fs"), P("fs", "tp"), P("fs", "tp"), P("fs", "tp")),
        out_specs=(P(None, "fs"), P(None, "fs"), P("fs", None), P("tp", "fs")),
        check_vma=False,
    )
```

profile of v0, /device:TPU:0, one launch (start us, length us, event | category | flops | bytes accessed | tf_op | source)
XLA Modules:
  0.0 524.6 jit_solution(6554279546055345411)
XLA Ops:
  7.2 0.0 all-gather.4.cloned.1.call-start
  7.2 5.5 %multiply_convert_fusion = (bf16[512,2816]{1,0:T(8,128)(2,1)S(1)}, bf16[512,2816]{1,0:T(8,128)(2,1)S(1)}) fusion(f32[512,2816]{1,0:T(8,128)} %param.8, f32[512]{0:T(512)} %param.6, f32[512,2816]{1,0:T(8,128)} %param.7), kind=kLoop, calls=%fused_computation | loop fusion | flops 5767168 | bytes 17303552 | tf_op jit(solution)/shard_map/convert_element_type | solution.py:10
  12.7 38.2 %all_to_all.64 = bf16[4,128,2816]{2,1,0:T(8,128)(2,1)} all-to-all(bf16[4,128,2816]{2,1,0:T(8,128)(2,1)S(1)} %bitcast.18), channel_id=1, replica_groups=mesh['fs'=8,'tp'=4] {'tp'}, dimensions={0} | all-to-all | bytes 5767168 | tf_op jit(solution)/shard_map/all_to_all | solution.py:14
  51.0 4.5 copy.9
  55.5 71.4 %all_to_all.65 = bf16[128,8,1408]{0,2,1:T(8,128)(2,1)} all-to-all(bf16[128,8,1408]{0,2,1:T(8,128)(2,1)} %bitcast.26), channel_id=1, replica_groups=mesh['fs'=8,'tp'=4] {'fs'}, dimensions={1} | all-to-all | bytes 5767168 | tf_op jit(solution)/shard_map/all_to_all | solution.py:18
  126.9 0.0 all-gather.4.cloned.1.call-update
  126.9 0.0 all-gather.6.cloned.1.call-start
  127.0 64.5 %all_to_all.66 = bf16[4,128,2816]{2,1,0:T(8,128)(2,1)} all-to-all(bf16[4,128,2816]{2,1,0:T(8,128)(2,1)S(1)} %bitcast.17), channel_id=1, replica_groups=mesh['fs'=8,'tp'=4] {'tp'}, dimensions={0} | all-to-all | bytes 5767168 | tf_op jit(solution)/shard_map/all_to_all | solution.py:15
  191.5 3.3 copy.11
  194.8 67.9 %all_to_all.67 = bf16[128,8,1408]{0,2,1:T(8,128)(2,1)} all-to-all(bf16[128,8,1408]{0,2,1:T(8,128)(2,1)S(1)} %bitcast.28), channel_id=1, replica_groups=mesh['fs'=8,'tp'=4] {'fs'}, dimensions={1} | all-to-all | bytes 5767168 | tf_op jit(solution)/shard_map/all_to_all | solution.py:19
  262.7 0.0 all-gather.6.cloned.1.call-update
  262.8 0.0 all-gather.8.cloned.1.call-start
  262.8 4.7 convert_element_type.26
  267.5 0.0 copy-start
  267.5 0.0 all-gather.8.cloned.1.call-update
  267.5 0.0 reduce-scatter.2.cloned.1.call-start
  267.6 1.6 copy-done
  269.1 0.4 fusion
  269.5 0.0 all-gather.4.cloned.1.call-done
  269.6 16.0 %copy.10 = bf16[8,512,1408]{2,1,0:T(8,128)(2,1)} copy(bf16[8,512,1408]{1,2,0:T(8,128)(2,1)} %all-gather.4.cloned.1.call-done) | data formatting | bytes 23068672 | tf_op jit(solution)/shard_map/all_gather | solution.py:24
  285.6 53.0 %all-gather.6.cloned.1.call-done = bf16[8,512,1408]{1,2,0:T(8,128)(2,1)} async-done(((bf16[8,128,1408]{1,2,0:T(8,128)(2,1)}), bf16[8,512,1408]{1,2,0:T(8,128)(2,1)}) %all-gather.6.cloned.1.call-update) | async-done | bytes 11534352 | tf_op jit(solution)/shard_map/all_gather | solution.py:25
  338.5 16.0 %copy.12 = bf16[8,512,1408]{2,1,0:T(8,128)(2,1)} copy(bf16[8,512,1408]{1,2,0:T(8,128)(2,1)} %all-gather.6.cloned.1.call-done) | data formatting | bytes 23068672 | tf_op jit(solution)/shard_map/all_gather | solution.py:25
  354.5 7.2 %fusion.3 = f32[1408,192]{0,1:T(8,128)S(1)} fusion(bf16[4096,1408]{1,0:T(8,128)(2,1)} %bitcast.19, bf16[192,4096]{1,0:T(8,128)(2,1)S(1)} %copy-done, f32[192]{0:T(256)S(1)} %add_rsqrt_fusion), kind=kOutput, calls=%fused_computation.9 | convolution fusion | flops 2216951808 | bytes 14189312 | tf_op jit(solution)/shard_map/dot_general | solution.py:33
  361.8 55.1 %all-gather.8.cloned.1.call-done = bf16[1408,4096]{1,0:T(8,128)(2,1)} async-done(((bf16[1408,1024]{1,0:T(8,128)(2,1)}), bf16[1408,4096]{1,0:T(8,128)(2,1)}) %all-gather.8.cloned.1.call-update) | async-done | bytes 11534352 | tf_op jit(solution)/shard_map/all_gather | solution.py:12
  416.8 14.4 %convolution_bitcast_fusion = f32[4096,192]{0,1:T(8,128)} fusion(bf16[1408,4096]{1,0:T(8,128)(2,1)} %all-gather.8.cloned.1.call-done, bf16[4096,1408]{1,0:T(8,128)(2,1)} %bitcast.21, f32[1408,192]{0,1:T(8,128)S(1)} %fusion.3, bf16[192,4096]{1,0:T(8,128)(2,1)S(1)} %copy-done, f32[192]{0:T(256)S(1)} %add_rsqrt_fusion), kind=kOutput, calls=%fused_computation.2 | convolution fusion | flops 4433166336 | bytes 28869376 | tf_op jit(solution)/shard_map/dot_general | solution.py:37
  431.3 0.0 reduce-scatter.2.cloned.1.call-update
  431.3 75.0 %reduce-scatter.2.cloned.1.call-done = f32[512,192]{0,1:T(8,128)} async-done(((f32[4096,192]{0,1:T(8,128)}), f32[512,192]{0,1:T(8,128)}) %reduce-scatter.2.cloned.1.call-update) | async-done | bytes 393232 | tf_op jit(solution)/shard_map/reduce_scatter | solution.py:36
  506.3 1.7 convert_bitcast_fusion
  508.0 10.1 %copy.14 = bf16[1408,4096]{1,0:T(8,128)(2,1)} copy(bf16[1408,4096]{1,0:T(8,128)(2,1)} %all-gather.8.cloned.1.call-done) | data formatting | bytes 23068672
  (1 shorter events, 0.0 us)
Async XLA Ops:
  7.2 262.4 %all-gather.4.cloned.1.call-start = ((), (), s32[]{:S(2)}) async-start(), calls=%async_computation.5 | async-start | bytes 14417920 | tf_op jit(solution)/shard_map/all_gather | solution.py:24
  126.9 211.6 %all-gather.6.cloned.1.call-start = ((), (), s32[]{:S(2)}) async-start(), calls=%async_computation.6 | async-start | bytes 14417920 | tf_op jit(solution)/shard_map/all_gather | solution.py:25
  262.8 154.1 %all-gather.8.cloned.1.call-start = ((), (), s32[]{:S(2)}) async-start(), calls=%async_computation.7 | async-start | bytes 14417920 | tf_op jit(solution)/shard_map/all_gather | solution.py:12
  267.5 1.6 copy-start
  267.5 238.8 %reduce-scatter.2.cloned.1.call-start = ((), (), s32[]{:S(2)}) async-start(), calls=%async_computation.8 | async-start | bytes 3538944 | tf_op jit(solution)/shard_map/reduce_scatter | solution.py:36
Sparse Core Ops, SparseCore 0:
  127.1 102.4 all-gather.3
  262.9 75.5 all-gather.5
  340.7 76.1 all-gather.7
  431.4 74.8 reduce-scatter.1
where the time goes:
time: 526 us; the launch traced here: 525 us
  blocking collectives  242 us (46%)
  waiting for transfers between devices  183 us (35%)
  local copies, waits for them, and re-layouts  51.5 us (10%)
  matrix products  21.7 us (4%)
  between operations  13.8 us (3%)
  other arithmetic  12.3 us (2%)
    reduce_scatter x1, waiting for transfers between devices, on_device(): lax.psum_scatter(lax.dot_general(down_serving, hidden_cols, (((0,), (0,))...  75 us
    all_to_all x1, blocking collectives, on_device(): lax.all_to_all(gate_part, 'fs', split_axis=1, concat_axis=0, tiled=True)  71.4 us
    all_to_all x1, blocking collectives, on_device(): lax.all_to_all(up_part, 'fs', split_axis=1, concat_axis=0, tiled=True)  67.9 us
    all_to_all x1, blocking collectives, on_device(): lax.all_to_all(up_cast, 'tp', split_axis=0, concat_axis=1, tiled=True)  64.5 us
    all_gather x1, waiting for transfers between devices, on_device(): down_serving = lax.all_gather(down_cast, 'tp', axis=1, tiled=True)  55.1 us
    all_gather x1, waiting for transfers between devices, on_device(): lax.all_gather(up_mid.reshape(fs_count, share, width), 'tp', axis=1, tile...  53 us
    all_to_all x1, blocking collectives, on_device(): lax.all_to_all(gate_cast, 'tp', split_axis=0, concat_axis=1, tiled=True)  38.2 us
    all_gather x1, local copies, waits for them, and re-layouts, on_device(): lax.all_gather(up_mid.reshape(fs_count, share, width), 'tp', axis=1, tile...  16 us
  transfers between devices with their start and end apart: 4, of which 3 were waited for; matrix products, arithmetic and copies ran while one was open for 9% of the time, Pallas kernels for 0%

commit v1 on v0

--- a/solution.py
+++ b/solution.py
@@ -2,6 +2,22 @@
 import jax.numpy as jnp
 from jax import lax
 from jax.sharding import PartitionSpec as P
+
+
+def swapped_with_each(shard, axis, split, join):
+    ways, here = (lax.axis_size(axis), lax.axis_index(axis))
+    width = shard.shape[split] // ways
+    shape = list(shard.shape)
+    shape[split] = width
+    height = shape[join]
+    shape[join] = height * ways
+    full = jnp.zeros(shape, shard.dtype)
+    for mask in range(ways):
+        part = lax.dynamic_slice_in_dim(shard, (here ^ mask) * width, width, axis=split)
+        if mask:
+            part = lax.ppermute(part, axis, [(d, d ^ mask) for d in range(ways)])
+        full = lax.dynamic_update_slice_in_dim(full, part, (here ^ mask) * height, axis=join)
+    return full
 
 
 def on_device(prompt_tokens, norm_gain, gate_trained, up_trained, down_trained):
@@ -15,7 +31,7 @@
         lax.all_to_all(up_cast, "tp", split_axis=0, concat_axis=1, tiled=True),
     )
     gate_mid, up_mid = (
-        lax.all_to_all(gate_part, "fs", split_axis=1, concat_axis=0, tiled=True),
+        swapped_with_each(gate_part, "fs", 1, 0),
         lax.all_to_all(up_part, "fs", split_axis=1, concat_axis=0, tiled=True),
     )
     share = gate_mid.shape[0] // fs_count

time: 526 us -> 542 us (1.030)
  blocking collectives: 242 us -> 137 us
  waiting for transfers between devices: 183 us -> 262 us
  local copies, waits for them, and re-layouts: 51.5 us -> 72.8 us
  starting transfers between devices: 0.16 us -> 17.9 us
    all_to_all x2 -> x0, blocking collectives: 110 us -> none  [the longest x1 71.4 us: on_device(): lax.all_to_all(gate_part, 'fs', split_axis=1, concat_axis=0, tiled=True)]
    all_to_all x0 -> x1, waiting for transfers between devices: none -> 34.7 us  [on_device(): lax.all_to_all(gate_cast, 'tp', split_axis=0, concat_axis=1, tiled=True)]
    ppermute x0 -> x7, waiting for transfers between devices: none -> 30.3 us  [swapped_with_each(): part = lax.ppermute(part, axis, [(d, d ^ mask) for d in range(ways)])]
    all_gather x1 -> x0, local copies, waits for them, and re-layouts: 16 us -> none  [on_device(): lax.all_gather(gate_mid.reshape(fs_count, share, width), 'tp', axis=1, ti...]
    ppermute x0 -> x7, starting transfers between devices: none -> 13 us  [swapped_with_each(): part = lax.ppermute(part, axis, [(d, d ^ mask) for d in range(ways)])]
    ppermute x0 -> x7, local copies, waits for them, and re-layouts: none -> 11.1 us  [swapped_with_each(): part = lax.ppermute(part, axis, [(d, d ^ mask) for d in range(ways)])]
    dynamic_update_slice x0 -> x8, local copies, waits for them, and re-layouts: none -> 10 us  [swapped_with_each(): lax.dynamic_update_slice_in_dim(full, part, (here ^ mask) * height, axis=...]
    unnamed x3 -> x4, local copies, waits for them, and re-layouts: 11.7 us -> 21.4 us
  transfers between devices with their start and end apart: 4 -> 12, of which waited for: 3 -> 7; matrix products, arithmetic and copies ran while one was open for 9% -> 10% of each run, Pallas kernels for 0% -> 0%
where the time goes in v1:
time: 542 us; the launch traced here: 541 us
  waiting for transfers between devices  262 us (48%)
  blocking collectives  137 us (25%)
  local copies, waits for them, and re-layouts  72.8 us (13%)
  matrix products  23.2 us (4%)
  starting transfers between devices  17.9 us (3%)
  between operations  13.9 us (3%)
  other arithmetic  13.8 us (3%)
    all_to_all x1, blocking collectives, on_device(): lax.all_to_all(up_part, 'fs', split_axis=1, concat_axis=0, tiled=True)  76.9 us
    reduce_scatter x1, waiting for transfers between devices, on_device(): lax.psum_scatter(lax.dot_general(down_serving, hidden_cols, (((0,), (0,))...  74.9 us
    all_gather x1, waiting for transfers between devices, on_device(): down_serving = lax.all_gather(down_cast, 'tp', axis=1, tiled=True)  62.3 us
    all_gather x1, waiting for transfers between devices, on_device(): lax.all_gather(up_mid.reshape(fs_count, share, width), 'tp', axis=1, tile...  60.2 us
    all_to_all x1, blocking collectives, on_device(): lax.all_to_all(up_cast, 'tp', split_axis=0, concat_axis=1, tiled=True)  59.9 us
    all_to_all x1, waiting for transfers between devices, on_device(): lax.all_to_all(gate_cast, 'tp', split_axis=0, concat_axis=1, tiled=True)  34.7 us
    ppermute x7, waiting for transfers between devices, swapped_with_each(): part = lax.ppermute(part, axis, [(d, d ^ mask) for d in range(ways)])  30.3 us
    unnamed x4, local copies, waits for them, and re-layouts  21.4 us
  transfers between devices with their start and end apart: 12, of which 7 were waited for; matrix products, arithmetic and copies ran while one was open for 10% of the time, Pallas kernels for 0%

profile of v1, /device:TPU:0, one launch (start us, length us, event | category | flops | bytes accessed | tf_op | source)
XLA Modules:
  0.0 540.9 jit_solution(3666838855310674838)
XLA Ops:
  7.2 7.1 %multiply_convert_fusion = (bf16[512,2816]{1,0:T(8,128)(2,1)S(1)}, bf16[512,2816]{1,0:T(8,128)(2,1)}) fusion(f32[512,2816]{1,0:T(8,128)} %param.8, f32[512]{0:T(512)} %param.6, f32[512,2816]{1,0:T(8,128)} %param.7), kind=kLoop, calls=%fused_computation | loop fusion | flops 5767168 | bytes 17303552 | tf_op jit(solution)/shard_map/convert_element_type | solution.py:26
  14.2 4.6 all-to-all-start
  18.9 0.0 all-gather.4.cloned.1.call-start
  19.0 34.7 %all-to-all-done = bf16[4,128,2816]{2,1,0:T(8,128)(2,1)} async-done(((bf16[4,128,2816]{2,1,0:T(8,128)(2,1)}), bf16[4,128,2816]{2,1,0:T(8,128)(2,1)}, u32[]{:S(2)}, u32[]{:S(2)}) %all-to-all-start) | async-done | bytes 2883616 | tf_op jit(solution)/shard_map/all_to_all | solution.py:30
  53.7 4.5 copy.9
  58.2 3.3 constant_dynamic-slice_fusion
  61.6 2.4 collective-permute-start
  63.9 1.6 collective-permute-start.1
  65.5 0.0 collective-permute-start.2
  65.5 3.0 collective-permute-start.3
  68.5 1.2 copy.10
  69.7 1.4 collective-permute-start.4
  71.0 1.8 broadcast_in_dim.2
  72.8 0.8 constant_dynamic-update-slice_fusion.7
  73.6 0.0 collective-permute-done
  73.6 3.6 collective-permute-start.5
  77.2 1.2 copy.11
  78.3 11.5 %collective-permute-done.1 = bf16[128,1408]{0,1:T(8,128)(2,1)} collective-permute-done((bf16[128,1408]{0,1:T(8,128)(2,1)}, bf16[128,1408]{0,1:T(8,128)(2,1)}, u32[]{:S(2)}, u32[]{:S(2)}) %collective-permute-start.1) | collective-permute-done | bytes 360480 | tf_op jit(solution)/shard_map/ppermute | solution.py:18
  89.9 1.1 collective-permute-start.6
  91.0 1.9 copy.12
  92.9 2.1 collective-permute-done.2
  95.0 1.9 copy.13
  96.9 0.0 collective-permute-done.3
  96.9 1.9 copy.14
  98.8 0.8 constant_dynamic-update-slice_fusion.6
  99.6 1.7 constant_dynamic-update-slice_fusion.5
  101.3 16.6 %collective-permute-done.4 = bf16[128,1408]{0,1:T(8,128)(2,1)} collective-permute-done((bf16[128,1408]{0,1:T(8,128)(2,1)}, bf16[128,1408]{0,1:T(8,128)(2,1)}, u32[]{:S(2)}, u32[]{:S(2)}) %collective-permute-start.4) | collective-permute-done | bytes 360480 | tf_op jit(solution)/shard_map/ppermute | solution.py:18
  118.0 1.2 copy.15
  119.1 1.8 constant_dynamic-update-slice_fusion.4
  120.9 1.7 constant_dynamic-update-slice_fusion.3
  122.6 0.0 collective-permute-done.5
  122.6 1.9 copy.16
  124.5 0.8 constant_dynamic-update-slice_fusion.2
  125.3 1.7 constant_dynamic-update-slice_fusion.1
  127.0 0.0 collective-permute-done.6
  127.0 1.2 copy.17
  128.2 0.8 constant_dynamic-update-slice_fusion
  129.0 0.0 all-gather.4.cloned.1.call-update
  129.0 0.0 all-gather.6.cloned.1.call-start
  129.1 59.9 %all_to_all.51 = bf16[4,128,2816]{2,1,0:T(8,128)(2,1)} all-to-all(bf16[4,128,2816]{2,1,0:T(8,128)(2,1)S(1)} %bitcast.17), channel_id=1, replica_groups=mesh['fs'=8,'tp'=4] {'tp'}, dimensions={0} | all-to-all | bytes 5767168 | tf_op jit(solution)/shard_map/all_to_all | solution.py:31
  189.0 3.3 copy.18
  192.4 76.9 %all_to_all.52 = bf16[128,8,1408]{0,2,1:T(8,128)(2,1)} all-to-all(bf16[128,8,1408]{0,2,1:T(8,128)(2,1)S(1)} %bitcast.26), channel_id=1, replica_groups=mesh['fs'=8,'tp'=4] {'fs'}, dimensions={1} | all-to-all | bytes 5767168 | tf_op jit(solution)/shard_map/all_to_all | solution.py:35
  269.3 0.0 all-gather.6.cloned.1.call-update
  269.3 0.0 all-gather.8.cloned.1.call-start
  269.3 4.7 convert_element_type.26
  274.0 0.0 copy-start
  274.0 0.0 all-gather.8.cloned.1.call-update
  274.0 0.2 reduce-scatter.2.cloned.1.call-start
  274.3 1.4 copy-done
  275.7 0.4 fusion
  276.1 0.0 all-gather.4.cloned.1.call-done
  276.1 8.7 %fusion.3 = f32[1408,192]{0,1:T(8,128)S(1)} fusion(bf16[4096,1408]{1,0:T(8,128)(2,1)} %bitcast.19, bf16[192,4096]{1,0:T(8,128)(2,1)S(1)} %copy-done, f32[192]{0:T(256)S(1)} %add_rsqrt_fusion), kind=kOutput, calls=%fused_computation.9 | convolution fusion | flops 2216951808 | bytes 14189312 | tf_op jit(solution)/shard_map/dot_general | solution.py:49
  284.8 60.2 %all-gather.6.cloned.1.call-done = bf16[8,512,1408]{1,2,0:T(8,128)(2,1)} async-done(((bf16[8,128,1408]{1,2,0:T(8,128)(2,1)}), bf16[8,512,1408]{1,2,0:T(8,128)(2,1)}) %all-gather.6.cloned.1.call-update) | async-done | bytes 11534352 | tf_op jit(solution)/shard_map/all_gather | solution.py:41
  345.0 16.0 %copy.19 = bf16[8,512,1408]{2,1,0:T(8,128)(2,1)} copy(bf16[8,512,1408]{1,2,0:T(8,128)(2,1)} %all-gather.6.cloned.1.call-done) | data formatting | bytes 23068672 | tf_op jit(solution)/shard_map/all_gather | solution.py:41
  361.1 62.3 %all-gather.8.cloned.1.call-done = bf16[1408,4096]{1,0:T(8,128)(2,1)} async-done(((bf16[1408,1024]{1,0:T(8,128)(2,1)}), bf16[1408,4096]{1,0:T(8,128)(2,1)}) %all-gather.8.cloned.1.call-update) | async-done | bytes 11534352 | tf_op jit(solution)/shard_map/all_gather | solution.py:28
  423.4 14.4 %convolution_bitcast_fusion = f32[4096,192]{0,1:T(8,128)} fusion(bf16[1408,4096]{1,0:T(8,128)(2,1)} %all-gather.8.cloned.1.call-done, bf16[4096,1408]{1,0:T(8,128)(2,1)} %bitcast.21, f32[1408,192]{0,1:T(8,128)S(1)} %fusion.3, bf16[192,4096]{1,0:T(8,128)(2,1)S(1)} %copy-done, f32[192]{0:T(256)S(1)} %add_rsqrt_fusion), kind=kOutput, calls=%fused_computation.2 | convolution fusion | flops 4433166336 | bytes 28869376 | tf_op jit(solution)/shard_map/dot_general | solution.py:53
  437.8 0.0 reduce-scatter.2.cloned.1.call-update
  437.8 74.9 %reduce-scatter.2.cloned.1.call-done = f32[512,192]{0,1:T(8,128)} async-done(((f32[4096,192]{0,1:T(8,128)}), f32[512,192]{0,1:T(8,128)}) %reduce-scatter.2.cloned.1.call-update) | async-done | bytes 393232 | tf_op jit(solution)/shard_map/reduce_scatter | solution.py:52
  512.7 1.7 convert_bitcast_fusion
  514.4 9.9 %copy.30 = bf16[4096,1408]{1,0:T(8,128)(2,1)} copy(bf16[4096,1408]{1,0:T(8,128)(2,1)} %bitcast.20) | data formatting | bytes 23068672
  524.3 10.1 %copy.31 = bf16[1408,4096]{1,0:T(8,128)(2,1)} copy(bf16[1408,4096]{1,0:T(8,128)(2,1)} %all-gather.8.cloned.1.call-done) | data formatting | bytes 23068672
  (1 shorter events, 0.0 us)
Async XLA Ops:
  14.2 39.4 %all-to-all-start = ((bf16[4,128,2816]{2,1,0:T(8,128)(2,1)}), bf16[4,128,2816]{2,1,0:T(8,128)(2,1)}, u32[]{:S(2)}, u32[]{:S(2)}) async-start(bf16[4,128,2816]{2,1,0:T(8,128)(2,1)} %bitcast.18), calls=%async_computation | async-start | bytes 5767168 | tf_op jit(solution)/shard_map/all_to_all | solution.py:30
  18.9 257.2 %all-gather.4.cloned.1.call-start = ((), (), s32[]{:S(2)}) async-start(), calls=%async_computation.4 | async-start | bytes 14417920 | tf_op jit(solution)/shard_map/all_gather | solution.py:40
  61.6 12.0 %collective-permute-start = (bf16[128,1408]{0,1:T(8,128)(2,1)}, bf16[128,1408]{0,1:T(8,128)(2,1)}, u32[]{:S(2)}, u32[]{:S(2)}) collective-permute-start(bf16[128,1408]{0,1:T(8,128)(2,1)} %get-tuple-element.10), channel_id=1, source_target_pairs={{0,4},{4,0},{8,12},{12,8},{16,20},{20,16},{24,28},{28,24},{1,5},{5... | collective-permute-start | bytes 1081352 | tf_op jit(solution)/shard_map/ppermute | solution.py:18
  63.9 26.0 %collective-permute-start.1 = (bf16[128,1408]{0,1:T(8,128)(2,1)}, bf16[128,1408]{0,1:T(8,128)(2,1)}, u32[]{:S(2)}, u32[]{:S(2)}) collective-permute-start(bf16[128,1408]{0,1:T(8,128)(2,1)} %get-tuple-element.9), channel_id=1, source_target_pairs={{0,8},{4,12},{8,0},{12,4},{16,24},{20,28},{24,16},{28,20},{1,9},{5... | collective-permute-start | bytes 1081352 | tf_op jit(solution)/shard_map/ppermute | solution.py:18
  65.5 29.5 %collective-permute-start.2 = (bf16[128,1408]{0,1:T(8,128)(2,1)}, bf16[128,1408]{0,1:T(8,128)(2,1)}, u32[]{:S(2)}, u32[]{:S(2)}) collective-permute-start(bf16[128,1408]{0,1:T(8,128)(2,1)} %get-tuple-element.8), channel_id=1, source_target_pairs={{0,12},{4,8},{8,4},{12,0},{16,28},{20,24},{24,20},{28,16},{1,13},{... | collective-permute-start | bytes 1081352 | tf_op jit(solution)/shard_map/ppermute | solution.py:18
  65.5 31.4 %collective-permute-start.3 = (bf16[128,1408]{0,1:T(8,128)(2,1)}, bf16[128,1408]{0,1:T(8,128)(2,1)}, u32[]{:S(2)}, u32[]{:S(2)}) collective-permute-start(bf16[128,1408]{0,1:T(8,128)(2,1)} %get-tuple-element.7), channel_id=1, source_target_pairs={{0,16},{4,20},{8,24},{12,28},{16,0},{20,4},{24,8},{28,12},{1,17},{... | collective-permute-start | bytes 1081352 | tf_op jit(solution)/shard_map/ppermute | solution.py:18
  69.7 48.3 %collective-permute-start.4 = (bf16[128,1408]{0,1:T(8,128)(2,1)}, bf16[128,1408]{0,1:T(8,128)(2,1)}, u32[]{:S(2)}, u32[]{:S(2)}) collective-permute-start(bf16[128,1408]{0,1:T(8,128)(2,1)} %get-tuple-element.6), channel_id=1, source_target_pairs={{0,20},{4,16},{8,28},{12,24},{16,4},{20,0},{24,12},{28,8},{1,21},{... | collective-permute-start | bytes 1081352 | tf_op jit(solution)/shard_map/ppermute | solution.py:18
  73.6 49.1 %collective-permute-start.5 = (bf16[128,1408]{0,1:T(8,128)(2,1)}, bf16[128,1408]{0,1:T(8,128)(2,1)}, u32[]{:S(2)}, u32[]{:S(2)}) collective-permute-start(bf16[128,1408]{0,1:T(8,128)(2,1)} %get-tuple-element.5), channel_id=1, source_target_pairs={{0,24},{4,28},{8,16},{12,20},{16,8},{20,12},{24,0},{28,4},{1,25},{... | collective-permute-start | bytes 1081352 | tf_op jit(solution)/shard_map/ppermute | solution.py:18
  89.9 37.2 %collective-permute-start.6 = (bf16[128,1408]{0,1:T(8,128)(2,1)}, bf16[128,1408]{0,1:T(8,128)(2,1)}, u32[]{:S(2)}, u32[]{:S(2)}) collective-permute-start(bf16[128,1408]{0,1:T(8,128)(2,1)} %get-tuple-element.4), channel_id=1, source_target_pairs={{0,28},{4,24},{8,20},{12,16},{16,12},{20,8},{24,4},{28,0},{1,29},{... | collective-permute-start | bytes 1081352 | tf_op jit(solution)/shard_map/ppermute | solution.py:18
  129.0 216.0 %all-gather.6.cloned.1.call-start = ((), (), s32[]{:S(2)}) async-start(), calls=%async_computation.5 | async-start | bytes 14417920 | tf_op jit(solution)/shard_map/all_gather | solution.py:41
  269.3 154.1 %all-gather.8.cloned.1.call-start = ((), (), s32[]{:S(2)}) async-start(), calls=%async_computation.6 | async-start | bytes 14417920 | tf_op jit(solution)/shard_map/all_gather | solution.py:28
  274.0 1.6 copy-start
  274.0 238.7 %reduce-scatter.2.cloned.1.call-start = ((), (), s32[]{:S(2)}) async-start(), calls=%async_computation.7 | async-start | bytes 3538944 | tf_op jit(solution)/shard_map/reduce_scatter | solution.py:52
Sparse Core Ops, SparseCore 0:
  129.1 100.9 all-gather.3
  269.4 75.5 all-gather.5
  347.2 76.1 all-gather.7
  437.9 74.7 reduce-scatter.1
